TPU v7x, 32 devices: a whole 2x2x4 slice. The times are simulated.
32 devices in a mesh: fs: 16 (over z, y, x), tp: 2 (over core).
Axes of the slice: x: 2, y: 2, z: 4, core: 2. Of those that a mesh axis runs over, the one named last changes fastest.
Arguments:
- tokens: bfloat16 [12288, 2048], P('fs'), may hold values from -6 to 6
- norm_gain: float32 [2048], replicated, may hold values from 0.1 to 1.9
- up_weight: float32 [2048, 8192], P('fs', 'tp'), may hold values from -0.125 to 0.125
- up_scale: float32 [8192], P('tp'), may hold values from 0.5 to 2
- down_weight: float32 [8192, 2048], P('tp', 'fs'), may hold values from -0.09375 to 0.09375
- down_scale: float32 [1, 2048], replicated, may hold values from 0.5 to 2
Outputs:
- mixed: bfloat16 [12288, 2048], P('fs', 'tp')
All inputs are finite; a program needn't handle non-finite values.
Results may differ from a plain program's by a relative error of at most 0.014.
Values may be sent and summed in bfloat16 or wider, within the bound.
A program may use at most 128 MiB of HBM per device.

v0:
```python
import functools

import jax
import jax.numpy as jnp
from jax import lax
from jax.experimental import pallas as pl
from jax.experimental.pallas import tpu as pltpu
from jax.sharding import PartitionSpec as P

MESH = pl.DeviceIdType.MESH
SIDE = 2
GROUP = SIDE * SIDE
CORES = 2
COLS = 256
STRIP = 32


def gathered(tokens, norm_gain, up_weight, up_scale, down_weight, down_scale):
    values = tokens.astype(jnp.float32)
    normed = (
        values * lax.rsqrt(jnp.mean(values * values, axis=-1, keepdims=True) + 1e-06) * norm_gain
    ).astype(jnp.bfloat16)
    up_cast = up_weight.astype(jnp.bfloat16)
    down_cast = down_weight.astype(jnp.bfloat16)
    up_full = lax.all_gather(up_cast, "fs", axis=0, tiled=True)
    pre = jnp.dot(normed, up_full, preferred_element_type=jnp.float32) * up_scale
    hidden = jnp.square(jnp.maximum(pre, 0.0)).astype(jnp.bfloat16)
    down_full = lax.all_gather(down_cast, "fs", axis=1, tiled=True)
    partial_value = jnp.dot(hidden, down_full, preferred_element_type=jnp.float32) * down_scale
    rounded = partial_value.astype(jnp.bfloat16)
    return (
        lax.psum_scatter(rounded, "tp", scatter_dimension=1, tiled=True)
        .astype(jnp.float32)
        .astype(jnp.bfloat16)
    )


def layer_kernel(
    layers, rows, tokens, gain, up_in, down_in, up_scale, down_scale, out,
    tok, upb, downb, hid, stage, partner, summed, peers, own,
    local_sem, piece_recv, piece_send, level_send, tok_recv, tok_send,
    mate_recv, mate_send, part_recv, part_send, red_recv, red_send,
):
    fs = lax.axis_index("fs")
    core = lax.axis_index("tp")
    z, q = fs // GROUP, fs % GROUP
    depth, width = up_in.shape[0], upb.shape[1]
    half = rows // CORES
    sub = half // 2
    units = 2 * layers
    per_layer = GROUP * depth // COLS
    per_unit = COLS // depth

    def at(r):
        return ((q // SIDE + r // SIDE) % SIDE) * SIDE + (q % SIDE + r % SIDE) % SIDE

    def chip(layer, inner):
        return (layer * GROUP + inner, core)

    mate = (fs, 1 - core)

    barrier = pltpu.get_barrier_semaphore()
    for r in range(1, GROUP):
        pl.semaphore_signal(barrier, inc=1, device_id=chip(z, at(r)), device_id_type=MESH)
    pl.semaphore_signal(barrier, inc=1, device_id=mate, device_id_type=MESH)

    @pl.when(z > 0)
    def _():
        pl.semaphore_signal(barrier, inc=1, device_id=chip(z - 1, q), device_id_type=MESH)

    @pl.when(z < layers - 1)
    def _():
        pl.semaphore_signal(barrier, inc=1, device_id=chip(z + 1, q), device_id_type=MESH)

    def slot(kind, layer, inner):
        if kind == 0:
            return upb.at[pl.ds(pl.multiple_of((layer * GROUP + inner) * depth, depth), depth), :]
        return downb.at[layer, :, pl.ds(pl.multiple_of(inner * depth, depth), depth)]

    def source(kind, inner):
        if kind == 0:
            return up_in.at[:, pl.ds(pl.multiple_of(inner * width, width), width)]
        return down_in.at[pl.ds(pl.multiple_of(inner * width, width), width), :]

    def remote(src, dst, send, recv, device):
        return pltpu.make_async_remote_copy(
            src_ref=src, dst_ref=dst, send_sem=send, recv_sem=recv,
            device_id=device, device_id_type=MESH,
        )

    def along(kind, layer, inner, way):
        piece = slot(kind, layer, inner)
        index = layer * GROUP + inner
        return remote(
            piece, piece, piece_send.at[kind, index, way], piece_recv.at[kind, index],
            chip(z + 2 * way - 1, q),
        )

    def level(kind, r):
        return remote(
            source(kind, at(r)), slot(kind, z, q), level_send.at[kind, r - 1],
            piece_recv.at[kind, fs], chip(z, at(r)),
        )

    def each_way(kind, layer, inner, act):
        @pl.when(jnp.logical_and(layer <= z, z < layers - 1))
        def _():
            act(along(kind, layer, inner, 1))

        @pl.when(jnp.logical_and(layer >= z, z > 0))
        def _():
            act(along(kind, layer, inner, 0))

    def start(copy):
        copy.start()

    def finish_send(copy):
        copy.wait_send()

    def arrived(kind, layer, inner):
        piece = slot(kind, layer, inner)
        remote(
            piece, piece, piece_send.at[kind, layer * GROUP + inner, 0],
            piece_recv.at[kind, layer * GROUP + inner], mate,
        ).wait_recv()

    def block(inner, side, s):
        return tok.at[pl.ds(pl.multiple_of(inner * rows + side * half + s * sub, sub), sub), :]

    def hand(r, s):
        piece = block(q, core, s)
        return remote(piece, piece, tok_send.at[r - 1, s], tok_recv.at[r - 1, s], chip(z, at(r)))

    def pass_on(came, to, s):
        piece = block(at(came), core, s)
        return remote(
            piece, piece, tok_send.at[GROUP - 2, s], tok_recv.at[GROUP - 2, s], chip(z, at(to))
        )

    def tok_arrived(r, s):
        piece = block(at(r), core, s)
        remote(piece, piece, tok_send.at[r - 1, s], tok_recv.at[r - 1, s], mate).wait_recv()

    def share(r, s):
        piece = block(at(r), core, s)
        return remote(piece, piece, mate_send.at[r, s], mate_recv.at[r, s], mate)

    half_at = pl.ds(pl.multiple_of(q * rows + core * half, half), half)
    mine_at = pl.ds(pl.multiple_of(core * half, half), half)
    locals_ = [
        pltpu.make_async_copy(source(0, q), slot(0, z, q), local_sem.at[0]),
        pltpu.make_async_copy(source(1, q), slot(1, z, q), local_sem.at[1]),
        pltpu.make_async_copy(tokens.at[mine_at, :], tok.at[half_at, :], local_sem.at[2]),
    ]
    for copy in locals_:
        copy.start()
    greeted = GROUP + jnp.where(z > 0, 1, 0) + jnp.where(z < layers - 1, 1, 0)
    pl.semaphore_wait(barrier, greeted)

    for r in (3, 1, 2):
        level(0, r).start()
    for copy in locals_:
        copy.wait()
    each_way(0, z, q, start)

    def normalize(i, carry):
        strip = pl.ds(pl.multiple_of(q * rows + core * half + i * STRIP, STRIP), STRIP)
        values = tok[strip, :].astype(jnp.float32)
        mean = jnp.mean(values * values, axis=-1, keepdims=True)
        tok[strip, :] = (values * lax.rsqrt(mean + 1e-06) * gain[...]).astype(tok.dtype)
        return carry

    lax.fori_loop(0, half // STRIP, normalize, 0)
    hand(1, 0).start()
    hand(2, 1).start()
    hand(1, 1).start()
    hand(2, 0).start()
    for r in (3, 1, 2):
        level(1, r).start()
    for s in (0, 1):
        share(0, s).start()
    for r in (1, 2, 3):
        arrived(0, z, at(r))
        each_way(0, z, at(r), start)

    def from_afar(d):
        for r in range(GROUP):
            @pl.when(z - d >= 0)
            def _():
                arrived(0, z - d, at(r))
                each_way(0, z - d, at(r), start)

            @pl.when(z + d < layers)
            def _():
                arrived(0, z + d, at(r))
                each_way(0, z + d, at(r), start)

    for d in range(1, layers):
        from_afar(d)
        if d == 1:
            tok_arrived(1, 0)
            pass_on(1, 2, 0).start()
            share(1, 0).start()
            tok_arrived(2, 1)
            pass_on(2, 1, 1).start()
            share(2, 1).start()
            for r in (1, 2, 3):
                arrived(1, z, at(r))
        for way, ahead in ((1, z), (0, layers - 1 - z)):
            due = ahead <= 1 if d == 1 else ahead == d

            @pl.when(jnp.logical_and(due, (layers - 1 - z if way else z) > 0))
            def _():
                for r in range(GROUP):
                    along(1, z, at(r), way).start()

    for r, s in ((1, 1), (2, 0), (3, 0), (3, 1)):
        tok_arrived(r, s)
        share(r, s).start()
    for r in (0, 1, 2, 3):
        for s in (0, 1):
            piece = block(at(r), 1 - core, s)
            remote(piece, piece, mate_send.at[r, s], mate_recv.at[r, s], mate).wait_recv()

    tall = rows * 2 // 3
    wide = 256
    across = width // wide

    def first(i, carry):
        m = pl.ds(pl.multiple_of((i // across) * tall, tall), tall)
        at_n = pl.multiple_of((i % across) * wide, wide)
        pre = jnp.dot(tok[m, :], upb[:, pl.ds(at_n, wide)], preferred_element_type=jnp.float32)
        pre = pre * up_scale[:, pl.ds(pl.multiple_of(q * width + at_n, wide), wide)]
        hid[m, pl.ds(at_n, wide)] = jnp.square(jnp.maximum(pre, 0.0)).astype(hid.dtype)
        return carry

    def take(d, r):
        for layer, there in ((z - d, z - d >= 0), (z + d, z + d < layers)):
            @pl.when(there)
            def _():
                arrived(1, layer, r)
                each_way(1, layer, r, start)

    inside = jnp.logical_and(z > 0, z < layers - 1)
    tiles = (GROUP * rows // tall) * across
    lax.fori_loop(0, tiles // 2, first, 0)

    @pl.when(inside)
    def _():
        for r in range(GROUP):
            take(1, r)

    lax.fori_loop(tiles // 2, tiles, first, 0)

    upper, lower = pl.ds(0, half), pl.ds(half, half)
    hops = ((3, upper, 2, 1), (3, lower, 2, 2), (1, upper, 0, 1), (2, lower, 1, 2),
            (1, lower, 0, 1), (2, upper, 1, 2))

    def red(u, k):
        of, part_rows, into, to = hops[k]
        return remote(
            summed.at[u, at(of), part_rows, :], peers.at[u, into, part_rows, :],
            red_send.at[u, k], red_recv.at[u, k], chip(z, at(to)),
        )

    def relay(u):
        for k, of, part_rows, then in ((0, 2, upper, 5), (1, 1, lower, 4)):
            red(u, k).wait_recv()
            total = summed[u, at(of), part_rows, :].astype(jnp.float32)
            total = total + peers[u, 2, part_rows, :].astype(jnp.float32)
            summed[u, at(of), part_rows, :] = total.astype(summed.dtype)
            red(u, then).start()

    def unit_of(t):
        s, h = t // per_layer, t % per_layer
        layer = jnp.where(
            2 * z < layers,
            jnp.where(s <= z, z - s, s),
            jnp.where(s <= layers - 1 - z, z + s, layers - 1 - s),
        )
        unit = layer * per_layer + h
        return s, h, layer, unit, unit // (units // CORES), unit % (units // CORES)

    def part(u, b):
        return remote(
            stage.at[u, b], partner.at[u, b], part_send.at[u, b], part_recv.at[u, b], mate
        )

    def second(t, carry):
        s, h, layer, unit, owner, u = unit_of(t)

        d = s + jnp.where(inside, 1, 0)

        @pl.when(d > jnp.where(inside, 1, 0))
        def _():
            for k in range(per_unit):
                take(d, h * per_unit + k)

        cols = pl.ds(pl.multiple_of(h * COLS, COLS), COLS)
        scale = pl.ds(pl.multiple_of(unit * COLS, COLS), COLS)

        def product(b):
            m = pl.ds(pl.multiple_of(b * rows, rows), rows)
            value = jnp.dot(hid[m, :], downb[layer, :, cols], preferred_element_type=jnp.float32)
            return value * down_scale[:, scale]

        @pl.when(owner != core)
        def _():
            def away(i, c):
                b = at(GROUP - 1 - i)
                stage[u, b] = product(b).astype(stage.dtype)
                part(u, b).start()
                return c

            lax.fori_loop(0, GROUP, away, 0)

        @pl.when(owner == core)
        def _():
            def mine(i, c):
                own[at(GROUP - 1 - i)] = product(at(GROUP - 1 - i))
                return c

            lax.fori_loop(0, GROUP, mine, 0)
            for r in (3, 2, 1, 0):
                b = at(r)
                part(u, b).wait_recv()
                summed[u, b] = (own[b] + partner[u, b].astype(jnp.float32)).astype(summed.dtype)
                for k in {3: (0, 1), 1: (2,), 2: (3,), 0: ()}[r]:
                    red(u, k).start()

        before = unit_of(jnp.maximum(t - 1, 0))

        @pl.when(jnp.logical_and(t > 0, before[4] == core))
        def _():
            relay(before[5])

        return carry

    lax.fori_loop(0, units, second, 0)
    final = unit_of(units - 1)

    @pl.when(final[4] == core)
    def _():
        relay(final[5])

    def last(u, carry):
        for k in range(2, 6):
            red(u, k).wait_recv()
        total = summed[u, q].astype(jnp.float32)
        for side in range(2):
            total = total + peers[u, side].astype(jnp.float32)
        out[:, pl.ds(pl.multiple_of(u * COLS, COLS), COLS)] = total.astype(out.dtype)
        return carry

    lax.fori_loop(0, units // CORES, last, 0)

    def drain(u, carry):
        for k in range(len(hops)):
            red(u, k).wait_send()
        for b in range(GROUP):
            part(u, b).wait_send()
        return carry

    lax.fori_loop(0, units // CORES, drain, 0)
    for kind in (0, 1):
        for r in range(1, GROUP):
            level(kind, r).wait_send()

        def drained(i, carry):
            each_way(kind, i // GROUP, i % GROUP, finish_send)
            return carry

        lax.fori_loop(0, layers * GROUP, drained, 0)
    for r in (1, 2):
        for s in (0, 1):
            hand(r, s).wait_send()
    pass_on(1, 2, 0).wait_send()
    pass_on(2, 1, 1).wait_send()
    for r in (0, 1, 2, 3):
        for s in (0, 1):
            share(r, s).wait_send()


def grouped(layers, tokens, norm_gain, up_weight, up_scale, down_weight, down_scale):
    up_cast = up_weight.astype(jnp.bfloat16)
    down_cast = down_weight.astype(jnp.bfloat16)
    rows, model = tokens.shape
    depth = up_weight.shape[0]
    width = up_weight.shape[1] // GROUP
    share = model // COLS // CORES
    n = layers * GROUP
    dma = pltpu.SemaphoreType.DMA
    vmem = pl.BlockSpec(memory_space=pltpu.VMEM)
    hbm = pl.BlockSpec(memory_space=pltpu.HBM)
    return pl.pallas_call(
        functools.partial(layer_kernel, layers, rows),
        out_shape=jax.ShapeDtypeStruct((rows, model // CORES), jnp.bfloat16),
        in_specs=[hbm, vmem, hbm, hbm, vmem, vmem],
        out_specs=vmem,
        scratch_shapes=[
            pltpu.VMEM((GROUP * rows, model), jnp.bfloat16),
            pltpu.VMEM((model, width), jnp.bfloat16),
            pltpu.VMEM((layers, width, GROUP * depth), jnp.bfloat16),
            pltpu.VMEM((GROUP * rows, width), jnp.bfloat16),
            pltpu.VMEM((share, GROUP, rows, COLS), jnp.bfloat16),
            pltpu.VMEM((share, GROUP, rows, COLS), jnp.bfloat16),
            pltpu.VMEM((share, GROUP, rows, COLS), jnp.bfloat16),
            pltpu.VMEM((share, GROUP - 1, rows, COLS), jnp.bfloat16),
            pltpu.VMEM((GROUP, rows, COLS), jnp.float32),
            dma((3,)),
            dma((2, n)),
            dma((2, n, 2)),
            dma((2, GROUP - 1)),
            dma((GROUP - 1, 2)),
            dma((GROUP - 1, 2)),
            dma((GROUP, 2)),
            dma((GROUP, 2)),
            dma((share, GROUP)),
            dma((share, GROUP)),
            dma((share, 6)),
            dma((share, 6)),
        ],
        compiler_params=pltpu.CompilerParams(
            collective_id=0, has_side_effects=True, vmem_limit_bytes=62 * 2**20
        ),
    )(tokens, norm_gain.reshape(1, -1), up_cast, down_cast, up_scale.reshape(1, -1), down_scale)


def solution(mesh):
    fs, tp = mesh.shape["fs"], mesh.shape["tp"]
    if tp == CORES and fs % (2 * GROUP) == 0 and fs <= 4 * GROUP:
        body = functools.partial(grouped, fs // GROUP)
    else:
        body = gathered
    in_specs = (P("fs", None), P(), P("fs", "tp"), P("tp"), P("tp", "fs"), P())
    out_specs = P("fs", "tp")
    return jax.shard_map(
        body, mesh=mesh, in_specs=in_specs, out_specs=out_specs, check_vma=False
    )
```

profile of v0, /device:TPU:1, one launch (start us, length us, event | category | flops | bytes accessed | tf_op | source)
XLA Modules:
  0.0 177.6 jit_solution(8349243237796239351)
XLA Ops:
  0.0 0.0 copy-start
  0.0 2.8 %convert_element_type.6.up_in = bf16[128,4096]{1,0:T(8,128)(2,1)} convert(f32[128,4096]{1,0:T(8,128)} %param.8) | non-fusion elementwise | flops 524288 | bytes 3145728 | tf_op jit(solution)/shard_map/convert_element_type | solution.py:385
  2.8 0.0 copy-done
  2.8 1.1 convert_element_type.7.down_in
  3.9 171.0 %shard_map.64 = bf16[768,1024]{1,0:T(8,128)(2,1)} custom-call(bf16[768,2048]{1,0:T(8,128)(2,1)} %tokens.1, f32[1,2048]{1,0:T(1,128)} %bitcast.3, bf16[128,4096]{1,0:T(8,128)(2,1)} %convert_element_type.6.up_in, bf16[4096,128]{1,0:T(8,128)(2,1)} %convert_element_type.7.down_in, f32[1,4096]{1,0:T(1,128)} %bitcast.2, f32[1,2048]{1,0:T(1,128)} %down_scale.1), custom_call_target="tpu_custom_call" | custom-call | tf_op jit(solution)/shard_map/pallas_call | solution.py:395
  174.9 2.7 %copy.8 = bf16[768,1024]{1,0:T(8,128)(2,1)} copy(bf16[768,1024]{1,0:T(8,128)(2,1)} %shard_map.64) | data formatting | bytes 3145728
Async XLA Ops:
  0.0 2.8 %copy-start = (f32[4096,128]{1,0:T(8,128)S(1)}, f32[4096,128]{1,0:T(8,128)}, u32[]{:S(2)}) copy-start(f32[4096,128]{1,0:T(8,128)} %param.10) | copy-start | bytes 6291460
where the time goes:
time: 178 us
  Pallas kernels  171 us (96%)
  other arithmetic  3.92 us (2%)
  local copies, waits for them, and re-layouts  2.67 us (2%)
    pallas_call x1, Pallas kernels, grouped(): pl.pallas_call(functools.partial(layer_kernel, layers, rows), out_shape=j...  171 us

commit v1 on v0

--- a/solution.py
+++ b/solution.py
@@ -38,8 +38,10 @@
 def layer_kernel(
     layers, rows, tokens, gain, up_in, down_in, up_scale, down_scale, out,
     tok, upb, downb, hid, stage, partner, summed, peers, own,
+    up_wide, down_wide, up_cast, down_cast,
     local_sem, piece_recv, piece_send, level_send, tok_recv, tok_send,
     mate_recv, mate_send, part_recv, part_send, red_recv, red_send,
+    end_part_recv, end_part_send, end_red_recv, end_red_send,
 ):
     fs = lax.axis_index("fs")
     core = lax.axis_index("tp")
@@ -78,9 +80,7 @@
         return downb.at[layer, :, pl.ds(pl.multiple_of(inner * depth, depth), depth)]
 
     def source(kind, inner):
-        if kind == 0:
-            return up_in.at[:, pl.ds(pl.multiple_of(inner * width, width), width)]
-        return down_in.at[pl.ds(pl.multiple_of(inner * width, width), width), :]
+        return (up_cast if kind == 0 else down_cast).at[inner]
 
     def remote(src, dst, send, recv, device):
         return pltpu.make_async_remote_copy(
@@ -147,21 +147,31 @@
 
     half_at = pl.ds(pl.multiple_of(q * rows + core * half, half), half)
     mine_at = pl.ds(pl.multiple_of(core * half, half), half)
-    locals_ = [
-        pltpu.make_async_copy(source(0, q), slot(0, z, q), local_sem.at[0]),
-        pltpu.make_async_copy(source(1, q), slot(1, z, q), local_sem.at[1]),
-        pltpu.make_async_copy(tokens.at[mine_at, :], tok.at[half_at, :], local_sem.at[2]),
-    ]
-    for copy in locals_:
-        copy.start()
+
+    def wide(kind, r):
+        part_at = pl.ds(pl.multiple_of(at(r) * width, width), width)
+        if kind == 0:
+            return pltpu.make_async_copy(up_in.at[:, part_at], up_wide.at[at(r)], local_sem.at[0, r])
+        return pltpu.make_async_copy(down_in.at[part_at, :], down_wide.at[at(r)], local_sem.at[1, r])
+
+    token_copy = pltpu.make_async_copy(tokens.at[mine_at, :], tok.at[half_at, :], local_sem.at[2, 0])
+    for r in range(GROUP):
+        wide(0, r).start()
+    token_copy.start()
+    for r in range(GROUP):
+        wide(1, r).start()
+    wide(0, 0).wait()
+    upb[pl.ds(pl.multiple_of(fs * depth, depth), depth), :] = up_wide[q].astype(upb.dtype)
+    for r in range(1, GROUP):
+        wide(0, r).wait()
+        up_cast[at(r)] = up_wide[at(r)].astype(up_cast.dtype)
+
     greeted = GROUP + jnp.where(z > 0, 1, 0) + jnp.where(z < layers - 1, 1, 0)
     pl.semaphore_wait(barrier, greeted)
 
-    for r in (3, 1, 2):
+    each_way(0, z, q, start)
+    for r in (1, 2, 3):
         level(0, r).start()
-    for copy in locals_:
-        copy.wait()
-    each_way(0, z, q, start)
 
     def normalize(i, carry):
         strip = pl.ds(pl.multiple_of(q * rows + core * half + i * STRIP, STRIP), STRIP)
@@ -170,69 +180,67 @@
         tok[strip, :] = (values * lax.rsqrt(mean + 1e-06) * gain[...]).astype(tok.dtype)
         return carry
 
+    token_copy.wait()
     lax.fori_loop(0, half // STRIP, normalize, 0)
     hand(1, 0).start()
     hand(2, 1).start()
     hand(1, 1).start()
     hand(2, 0).start()
-    for r in (3, 1, 2):
+    wide(1, 0).wait()
+    downb[z, :, pl.ds(pl.multiple_of(q * depth, depth), depth)] = down_wide[q].astype(downb.dtype)
+    for r in range(1, GROUP):
+        wide(1, r).wait()
+        down_cast[at(r)] = down_wide[at(r)].astype(down_cast.dtype)
+    for r in (1, 2, 3):
         level(1, r).start()
     for s in (0, 1):
         share(0, s).start()
-    for r in (1, 2, 3):
+
+    inside = jnp.logical_and(z > 0, z < layers - 1)
+
+    def near(r):
         arrived(0, z, at(r))
         each_way(0, z, at(r), start)
 
-    def from_afar(d):
-        for r in range(GROUP):
-            @pl.when(z - d >= 0)
+    def afar(d, r):
+        for layer, there in ((z - d, z - d >= 0), (z + d, z + d < layers)):
+            @pl.when(there)
             def _():
-                arrived(0, z - d, at(r))
-                each_way(0, z - d, at(r), start)
-
-            @pl.when(z + d < layers)
-            def _():
-                arrived(0, z + d, at(r))
-                each_way(0, z + d, at(r), start)
-
-    for d in range(1, layers):
-        from_afar(d)
-        if d == 1:
-            tok_arrived(1, 0)
-            pass_on(1, 2, 0).start()
-            share(1, 0).start()
-            tok_arrived(2, 1)
-            pass_on(2, 1, 1).start()
-            share(2, 1).start()
-            for r in (1, 2, 3):
-                arrived(1, z, at(r))
-        for way, ahead in ((1, z), (0, layers - 1 - z)):
-            due = ahead <= 1 if d == 1 else ahead == d
-
-            @pl.when(jnp.logical_and(due, (layers - 1 - z if way else z) > 0))
-            def _():
-                for r in range(GROUP):
-                    along(1, z, at(r), way).start()
-
-    for r, s in ((1, 1), (2, 0), (3, 0), (3, 1)):
+                arrived(0, layer, at(r))
+                each_way(0, layer, at(r), start)
+
+    def when_inside(d, rs):
+        @pl.when(inside)
+        def _():
+            for r in rs:
+                afar(d, r)
+
+    near(1)
+    near(2)
+    when_inside(1, (0,))
+    near(3)
+    when_inside(1, (1, 2, 3))
+    tok_arrived(1, 0)
+    pass_on(1, 2, 0).start()
+    share(1, 0).start()
+    tok_arrived(2, 1)
+    pass_on(2, 1, 1).start()
+    share(2, 1).start()
+    for d in range(2, layers):
+        when_inside(d, range(GROUP))
+    for r, s in ((1, 1), (2, 0)):
         tok_arrived(r, s)
         share(r, s).start()
-    for r in (0, 1, 2, 3):
-        for s in (0, 1):
-            piece = block(at(r), 1 - core, s)
-            remote(piece, piece, mate_send.at[r, s], mate_recv.at[r, s], mate).wait_recv()
-
-    tall = rows * 2 // 3
-    wide = 256
-    across = width // wide
-
-    def first(i, carry):
-        m = pl.ds(pl.multiple_of((i // across) * tall, tall), tall)
-        at_n = pl.multiple_of((i % across) * wide, wide)
-        pre = jnp.dot(tok[m, :], upb[:, pl.ds(at_n, wide)], preferred_element_type=jnp.float32)
-        pre = pre * up_scale[:, pl.ds(pl.multiple_of(q * width + at_n, wide), wide)]
-        hid[m, pl.ds(at_n, wide)] = jnp.square(jnp.maximum(pre, 0.0)).astype(hid.dtype)
-        return carry
+    for r in (1, 2, 3):
+        arrived(1, z, at(r))
+    for i in range(GROUP):
+        each_way(1, z, i, start)
+
+    @pl.when(jnp.logical_not(inside))
+    def _():
+        for d in range(1, layers):
+            for r in range(GROUP):
+                afar(d, r)
 
     def take(d, r):
         for layer, there in ((z - d, z - d >= 0), (z + d, z + d < layers)):
@@ -241,16 +249,39 @@
                 arrived(1, layer, r)
                 each_way(1, layer, r, start)
 
-    inside = jnp.logical_and(z > 0, z < layers - 1)
-    tiles = (GROUP * rows // tall) * across
-    lax.fori_loop(0, tiles // 2, first, 0)
+    wide_n = COLS
+    across = width // wide_n
+    turn = jnp.where(inside, GROUP - 1, GROUP - 2)
+
+    def first(i, carry):
+        r = i // across
+        b = at(r)
+
+        @pl.when(i == turn * across)
+        def _():
+            for s in (0, 1):
+                tok_arrived(3, s)
+                share(3, s).start()
+
+        @pl.when(i % across == 0)
+        def _():
+            for s in (0, 1):
+                piece = block(b, 1 - core, s)
+                remote(piece, piece, mate_send.at[r, s], mate_recv.at[r, s], mate).wait_recv()
+
+        m = pl.ds(pl.multiple_of(b * rows, rows), rows)
+        at_n = pl.multiple_of((i % across) * wide_n, wide_n)
+        pre = jnp.dot(tok[m, :], upb[:, pl.ds(at_n, wide_n)], preferred_element_type=jnp.float32)
+        pre = pre * up_scale[:, pl.ds(pl.multiple_of(q * width + at_n, wide_n), wide_n)]
+        hid[m, pl.ds(at_n, wide_n)] = jnp.square(jnp.maximum(pre, 0.0)).astype(hid.dtype)
+        return carry
+
+    lax.fori_loop(0, GROUP * across, first, 0)
 
     @pl.when(inside)
     def _():
         for r in range(GROUP):
             take(1, r)
-
-    lax.fori_loop(tiles // 2, tiles, first, 0)
 
     upper, lower = pl.ds(0, half), pl.ds(half, half)
     hops = ((3, upper, 2, 1), (3, lower, 2, 2), (1, upper, 0, 1), (2, lower, 1, 2),
@@ -289,12 +320,10 @@
     def second(t, carry):
         s, h, layer, unit, owner, u = unit_of(t)
 
-        d = s + jnp.where(inside, 1, 0)
-
-        @pl.when(d > jnp.where(inside, 1, 0))
+        @pl.when(s > jnp.where(inside, 1, 0))
         def _():
             for k in range(per_unit):
-                take(d, h * per_unit + k)
+                take(s, h * per_unit + k)
 
         cols = pl.ds(pl.multiple_of(h * COLS, COLS), COLS)
         scale = pl.ds(pl.multiple_of(unit * COLS, COLS), COLS)
@@ -336,32 +365,124 @@
 
         return carry
 
-    lax.fori_loop(0, units, second, 0)
-    final = unit_of(units - 1)
-
-    @pl.when(final[4] == core)
-    def _():
-        relay(final[5])
+    lax.fori_loop(0, units - 1, second, 0)
+    before = unit_of(units - 2)
+
+    @pl.when(before[4] == core)
+    def _():
+        relay(before[5])
+
+    s_end, h_end, layer_end, unit_end, owner_end, u_end = unit_of(units - 1)
+    mine_end = owner_end == core
+    thin = COLS // 2
+
+    def end_part(e, r):
+        piece = pl.ds(e * thin, thin)
+        return remote(
+            stage.at[u_end, at(r), :, piece], partner.at[u_end, at(r), :, piece],
+            end_part_send.at[e, r], end_part_recv.at[e, r], mate,
+        )
+
+    def end_red(e, r):
+        piece = pl.ds(e * thin, thin)
+        return remote(
+            summed.at[u_end, at(r), :, piece], peers.at[u_end, r - 1, :, piece],
+            end_red_send.at[e, r - 1], end_red_recv.at[e, r - 1], chip(z, at(r)),
+        )
+
+    for e in range(2):
+        @pl.when(s_end > jnp.where(inside, 1, 0))
+        def _():
+            for k in ((e,) if per_unit == 2 else range(per_unit * (1 - e))):
+                take(s_end, h_end * per_unit + k)
+
+        piece = pl.ds(e * thin, thin)
+        cols = pl.ds(pl.multiple_of(h_end * COLS + e * thin, thin), thin)
+        scale = pl.ds(pl.multiple_of(unit_end * COLS + e * thin, thin), thin)
+
+        def product(r):
+            m = pl.ds(pl.multiple_of(at(r) * rows, rows), rows)
+            value = jnp.dot(
+                hid[m, :], downb[layer_end, :, cols], preferred_element_type=jnp.float32
+            )
+            return value * down_scale[:, scale]
+
+        @pl.when(jnp.logical_not(mine_end))
+        def _():
+            for r in (3, 1, 2, 0):
+                stage[u_end, at(r), :, piece] = product(r).astype(stage.dtype)
+                end_part(e, r).start()
+
+        @pl.when(mine_end)
+        def _():
+            def gather(r):
+                end_part(e, r).wait_recv()
+                total = own[r, :, piece] + partner[u_end, at(r), :, piece].astype(jnp.float32)
+                summed[u_end, at(r), :, piece] = total.astype(summed.dtype)
+                if r:
+                    end_red(e, r).start()
+
+            order = (3, 1, 2, 0)
+            for i, r in enumerate(order):
+                own[r, :, piece] = product(r)
+                if i > 1:
+                    gather(order[i - 2])
+            gather(order[2])
+            gather(order[3])
 
     def last(u, carry):
-        for k in range(2, 6):
-            red(u, k).wait_recv()
-        total = summed[u, q].astype(jnp.float32)
-        for side in range(2):
-            total = total + peers[u, side].astype(jnp.float32)
-        out[:, pl.ds(pl.multiple_of(u * COLS, COLS), COLS)] = total.astype(out.dtype)
+        @pl.when(jnp.logical_not(jnp.logical_and(mine_end, u == u_end)))
+        def _():
+            for k in range(2, 6):
+                red(u, k).wait_recv()
+            total = summed[u, q].astype(jnp.float32)
+            for side in range(2):
+                total = total + peers[u, side].astype(jnp.float32)
+            out[:, pl.ds(pl.multiple_of(u * COLS, COLS), COLS)] = total.astype(out.dtype)
+
         return carry
 
     lax.fori_loop(0, units // CORES, last, 0)
 
+    @pl.when(mine_end)
+    def _():
+        for e in range(2):
+            piece = pl.ds(e * thin, thin)
+            for r in (1, 2, 3):
+                end_red(e, r).wait_recv()
+            total = summed[u_end, q, :, piece].astype(jnp.float32)
+            for side in range(3):
+                total = total + peers[u_end, side, :, piece].astype(jnp.float32)
+            to = pl.ds(pl.multiple_of(u_end * COLS + e * thin, thin), thin)
+            out[:, to] = total.astype(out.dtype)
+
     def drain(u, carry):
-        for k in range(len(hops)):
-            red(u, k).wait_send()
-        for b in range(GROUP):
-            part(u, b).wait_send()
+        @pl.when(jnp.logical_not(jnp.logical_and(mine_end, u == u_end)))
+        def _():
+            for k in range(len(hops)):
+                red(u, k).wait_send()
+
+        @pl.when(jnp.logical_or(mine_end, u != u_end))
+        def _():
+            for b in range(GROUP):
+                part(u, b).wait_send()
+
         return carry
 
     lax.fori_loop(0, units // CORES, drain, 0)
+
+    @pl.when(mine_end)
+    def _():
+        for e in range(2):
+            for r in (1, 2, 3):
+                end_red(e, r).wait_send()
+
+    @pl.when(jnp.logical_not(mine_end))
+    def _():
+        for e in range(2):
+            for r in range(GROUP):
+                end_part(e, r).wait_send()
+
     for kind in (0, 1):
         for r in range(1, GROUP):
             level(kind, r).wait_send()
@@ -382,8 +503,6 @@
 
 
 def grouped(layers, tokens, norm_gain, up_weight, up_scale, down_weight, down_scale):
-    up_cast = up_weight.astype(jnp.bfloat16)
-    down_cast = down_weight.astype(jnp.bfloat16)
     rows, model = tokens.shape
     depth = up_weight.shape[0]
     width = up_weight.shape[1] // GROUP
@@ -394,7 +513,7 @@
     hbm = pl.BlockSpec(memory_space=pltpu.HBM)
     return pl.pallas_call(
         functools.partial(layer_kernel, layers, rows),
-        out_shape=jax.ShapeDtypeStruct((rows, model // CORES), jnp.bfloat16),
+        out_shape=pltpu.VMEM((rows, model // CORES), jnp.bfloat16),
         in_specs=[hbm, vmem, hbm, hbm, vmem, vmem],
         out_specs=vmem,
         scratch_shapes=[
@@ -407,7 +526,11 @@
             pltpu.VMEM((share, GROUP, rows, COLS), jnp.bfloat16),
             pltpu.VMEM((share, GROUP - 1, rows, COLS), jnp.bfloat16),
             pltpu.VMEM((GROUP, rows, COLS), jnp.float32),
-            dma((3,)),
+            pltpu.VMEM((GROUP, depth, width), jnp.float32),
+            pltpu.VMEM((GROUP, width, depth), jnp.float32),
+            pltpu.VMEM((GROUP, depth, width), jnp.bfloat16),
+            pltpu.VMEM((GROUP, width, depth), jnp.bfloat16),
+            dma((3, GROUP)),
             dma((2, n)),
             dma((2, n, 2)),
             dma((2, GROUP - 1)),
@@ -419,11 +542,17 @@
             dma((share, GROUP)),
             dma((share, 6)),
             dma((share, 6)),
+            dma((2, GROUP)),
+            dma((2, GROUP)),
+            dma((2, GROUP - 1)),
+            dma((2, GROUP - 1)),
         ],
         compiler_params=pltpu.CompilerParams(
-            collective_id=0, has_side_effects=True, vmem_limit_bytes=62 * 2**20
+            collective_id=0, has_side_effects=True, vmem_limit_bytes=60 * 2**20
         ),
-    )(tokens, norm_gain.reshape(1, -1), up_cast, down_cast, up_scale.reshape(1, -1), down_scale)
+    )(
+        tokens, norm_gain.reshape(1, -1), up_weight, down_weight, up_scale.reshape(1, -1), down_scale
+    )
 
 
 def solution(mesh):

time: 178 us -> 159 us (0.89)
  Pallas kernels: 171 us -> 157 us
  other arithmetic: 3.92 us -> 0 us
    pallas_call x1, Pallas kernels: 171 us -> 157 us  [grouped(): pl.pallas_call(functools.partial(layer_kernel, layers, rows), out_shape=p...]
    convert_element_type x2 -> x0, other arithmetic: 3.92 us -> none  [the longest x1 2.84 us: grouped(): up_cast = up_weight.astype(jnp.bfloat16)]
where the time goes in v1:
time: 159 us
  Pallas kernels  157 us (99%)
    pallas_call x1, Pallas kernels, grouped(): pl.pallas_call(functools.partial(layer_kernel, layers, rows), out_shape=p...  157 us

profile of v1, /device:TPU:1, one launch (start us, length us, event | category | flops | bytes accessed | tf_op | source)
XLA Modules:
  0.0 158.6 jit_solution(572089997499348883)
XLA Ops:
  0.0 157.5 %shard_map.64 = bf16[768,1024]{1,0:T(8,128)(2,1)S(1)} custom-call(bf16[768,2048]{1,0:T(8,128)(2,1)} %tokens.1, f32[1,2048]{1,0:T(1,128)} %bitcast.3, f32[128,4096]{1,0:T(8,128)} %up_in.1, f32[4096,128]{1,0:T(8,128)} %down_in.1, f32[1,4096]{1,0:T(1,128)} %bitcast.2, f32[1,2048]{1,0:T(1,128)} %down_scale.1), custom_call_target="tpu_custom_call" | custom-call | tf_op jit(solution)/shard_map/pallas_call | solution.py:514
  157.5 1.1 copy.8

commit v2 on v1

v2 whole, which is shorter than its diff:
```python
import functools

import jax
import jax.numpy as jnp
from jax import lax
from jax.experimental import pallas as pl
from jax.experimental.pallas import tpu as pltpu
from jax.sharding import PartitionSpec as P

MESH = pl.DeviceIdType.MESH
SIDE = 2
GROUP = SIDE * SIDE
CORES = 2
COLS = 256
STRIP = 32


def gathered(tokens, norm_gain, up_weight, up_scale, down_weight, down_scale):
    values = tokens.astype(jnp.float32)
    normed = (
        values * lax.rsqrt(jnp.mean(values * values, axis=-1, keepdims=True) + 1e-06) * norm_gain
    ).astype(jnp.bfloat16)
    up_cast = up_weight.astype(jnp.bfloat16)
    down_cast = down_weight.astype(jnp.bfloat16)
    up_full = lax.all_gather(up_cast, "fs", axis=0, tiled=True)
    pre = jnp.dot(normed, up_full, preferred_element_type=jnp.float32) * up_scale
    hidden = jnp.square(jnp.maximum(pre, 0.0)).astype(jnp.bfloat16)
    down_full = lax.all_gather(down_cast, "fs", axis=1, tiled=True)
    partial_value = jnp.dot(hidden, down_full, preferred_element_type=jnp.float32) * down_scale
    rounded = partial_value.astype(jnp.bfloat16)
    return (
        lax.psum_scatter(rounded, "tp", scatter_dimension=1, tiled=True)
        .astype(jnp.float32)
        .astype(jnp.bfloat16)
    )


def layer_kernel(
    layers, rows, tokens, gain_in, up_in, down_in, up_scale_in, down_scale_in, out,
    gain, up_scale, down_scale, tok, upb, downb, hid, stage, partner, summed, peers, own,
    up_wide, down_wide, up_cast, down_cast,
    local_sem, piece_recv, piece_send, level_send, near_recv, tok_recv, mate_recv,
    part_recv, red_recv, end_red_recv, sent,
):
    fs = lax.axis_index("fs")
    core = lax.axis_index("tp")
    z, q = fs // GROUP, fs % GROUP
    depth, width = up_in.shape[0], upb.shape[1]
    half = rows // CORES
    sub = half // 2
    units = 2 * layers
    per_layer = GROUP * depth // COLS
    per_unit = COLS // depth

    def at(r):
        return ((q // SIDE + r // SIDE) % SIDE) * SIDE + (q % SIDE + r % SIDE) % SIDE

    def chip(layer, inner):
        return (layer * GROUP + inner, core)

    mate = (fs, 1 - core)

    barrier = pltpu.get_barrier_semaphore()
    for r in range(1, GROUP):
        pl.semaphore_signal(barrier, inc=1, device_id=chip(z, at(r)), device_id_type=MESH)
    pl.semaphore_signal(barrier, inc=1, device_id=mate, device_id_type=MESH)

    @pl.when(z > 0)
    def _():
        pl.semaphore_signal(barrier, inc=1, device_id=chip(z - 1, q), device_id_type=MESH)

    @pl.when(z < layers - 1)
    def _():
        pl.semaphore_signal(barrier, inc=1, device_id=chip(z + 1, q), device_id_type=MESH)

    def slot(kind, layer, inner):
        if kind == 0:
            return upb.at[pl.ds(pl.multiple_of((layer * GROUP + inner) * depth, depth), depth), :]
        return downb.at[layer, :, pl.ds(pl.multiple_of(inner * depth, depth), depth)]

    tok_send, mate_send, part_send, red_send = (sent.at[i] for i in range(4))

    def source(kind, inner):
        return (up_cast if kind == 0 else down_cast).at[inner]

    def remote(src, dst, send, recv, device):
        return pltpu.make_async_remote_copy(
            src_ref=src, dst_ref=dst, send_sem=send, recv_sem=recv,
            device_id=device, device_id_type=MESH,
        )

    def along(kind, layer, inner, way):
        piece = slot(kind, layer, inner)
        index = layer * GROUP + inner
        return remote(
            piece, piece, piece_send.at[kind, way], piece_recv.at[kind, index],
            chip(z + 2 * way - 1, q),
        )

    def level(r):
        return remote(
            source(1, at(r)), slot(1, z, q), level_send.at[1],
            piece_recv.at[1, fs], chip(z, at(r)),
        )

    def first_rows(h, inner=q):
        lower = (z * GROUP + inner) * depth + h * (depth // 2)
        return upb.at[pl.ds(pl.multiple_of(lower, depth // 2), depth // 2), :]

    def near_half(r, h):
        return remote(
            source(0, at(r)).at[pl.ds(h * (depth // 2), depth // 2), :], first_rows(h),
            level_send.at[0], near_recv.at[r - 1, h], chip(z, at(r)),
        )

    def half_along(inner, way, h):
        piece = first_rows(h, inner)
        index = z * GROUP + inner
        return remote(
            piece, piece, piece_send.at[0, way], piece_recv.at[0, index],
            chip(z + 2 * way - 1, q),
        )

    def each_way(kind, layer, inner, act):
        @pl.when(jnp.logical_and(layer <= z, z < layers - 1))
        def _():
            act(along(kind, layer, inner, 1))

        @pl.when(jnp.logical_and(layer >= z, z > 0))
        def _():
            act(along(kind, layer, inner, 0))

    def start(copy):
        copy.start()

    def finish_send(copy):
        copy.wait_send()

    def arrived(kind, layer, inner):
        piece = slot(kind, layer, inner)
        remote(
            piece, piece, piece_send.at[kind, 0],
            piece_recv.at[kind, layer * GROUP + inner], mate,
        ).wait_recv()

    def block(inner, side, s):
        return tok.at[pl.ds(pl.multiple_of(inner * rows + side * half + s * sub, sub), sub), :]

    def hand(r, s):
        piece = block(q, core, s)
        return remote(piece, piece, tok_send, tok_recv.at[r - 1, s], chip(z, at(r)))

    def pass_on(came, to, s):
        piece = block(at(came), core, s)
        return remote(
            piece, piece, tok_send, tok_recv.at[GROUP - 2, s], chip(z, at(to))
        )

    def tok_arrived(r, s):
        piece = block(at(r), core, s)
        remote(piece, piece, tok_send, tok_recv.at[r - 1, s], mate).wait_recv()

    def share(r, s):
        piece = block(at(r), core, s)
        return remote(piece, piece, mate_send, mate_recv.at[r], mate)

    half_at = pl.ds(pl.multiple_of(q * rows + core * half, half), half)
    mine_at = pl.ds(pl.multiple_of(core * half, half), half)

    down_copy = pltpu.make_async_copy(down_in, down_wide, local_sem.at[1])
    token_copy = pltpu.make_async_copy(tokens.at[mine_at, :], tok.at[half_at, :], local_sem.at[2])
    small = [
        pltpu.make_async_copy(gain_in, gain, local_sem.at[3]),
        pltpu.make_async_copy(up_scale_in, up_scale, local_sem.at[4]),
        pltpu.make_async_copy(down_scale_in, down_scale, local_sem.at[5]),
    ]

    def part_at(r):
        return pl.ds(pl.multiple_of(at(r) * width, width), width)

    def up_copy(r):
        return pltpu.make_async_copy(
            up_in.at[:, part_at(r)], up_wide.at[:, part_at(r)], local_sem.at[6 if r else 0]
        )

    for r in range(GROUP):
        up_copy(r).start()
    token_copy.start()
    for copy in small:
        copy.start()
    down_copy.start()
    up_copy(0).wait()
    own_rows = pl.ds(pl.multiple_of(fs * depth, depth), depth)
    upb[own_rows, :] = up_wide[:, part_at(0)].astype(upb.dtype)
    greeted = GROUP + jnp.where(z > 0, 1, 0) + jnp.where(z < layers - 1, 1, 0)
    pl.semaphore_wait(barrier, greeted)
    each_way(0, z, q, start)
    others = up_wide.at[:, pl.ds(0, (GROUP - 1) * width)]
    pltpu.make_async_copy(others, others, local_sem.at[6]).wait()
    for r in range(1, GROUP):
        up_cast[at(r)] = up_wide[:, part_at(r)].astype(up_cast.dtype)

    for r in (1, 2, 3):
        for h in (0, 1):
            near_half(r, h).start()

    def normalize(i, carry):
        strip = pl.ds(pl.multiple_of(q * rows + core * half + i * STRIP, STRIP), STRIP)
        values = tok[strip, :].astype(jnp.float32)
        mean = jnp.mean(values * values, axis=-1, keepdims=True)
        tok[strip, :] = (values * lax.rsqrt(mean + 1e-06) * gain[...]).astype(tok.dtype)
        return carry

    token_copy.wait()
    small[0].wait()
    lax.fori_loop(0, half // STRIP, normalize, 0)

    hand(1, 0).start()
    hand(2, 1).start()
    hand(1, 1).start()
    hand(2, 0).start()
    down_copy.wait()
    own_cols = pl.ds(pl.multiple_of(q * depth, depth), depth)
    downb[z, :, own_cols] = down_wide[part_at(0), :].astype(downb.dtype)
    for r in range(1, GROUP):
        down_cast[at(r)] = down_wide[part_at(r), :].astype(down_cast.dtype)
    for r in (1, 2, 3):
        level(r).start()
    for s in (0, 1):
        share(0, s).start()

    inside = jnp.logical_and(z > 0, z < layers - 1)

    def near(r, h):
        piece = first_rows(h, at(r))
        remote(piece, piece, level_send.at[0], near_recv.at[r - 1, h], mate).wait_recv()

        @pl.when(z < layers - 1)
        def _():
            half_along(at(r), 1, h).start()

        @pl.when(z > 0)
        def _():
            half_along(at(r), 0, h).start()

    def afar(d, r):
        for layer, there in ((z - d, z - d >= 0), (z + d, z + d < layers)):
            @pl.when(there)
            def _():
                arrived(0, layer, at(r))
                each_way(0, layer, at(r), start)

    def when_inside(d, rs):
        @pl.when(inside)
        def _():
            for r in rs:
                afar(d, r)

    for h in (0, 1):
        for r in (1, 2):
            near(r, h)
    when_inside(1, (0,))
    for h in (0, 1):
        near(3, h)
    when_inside(1, (1, 2, 3))
    tok_arrived(1, 0)
    pass_on(1, 2, 0).start()
    share(1, 0).start()
    tok_arrived(2, 1)
    pass_on(2, 1, 1).start()
    share(2, 1).start()
    for d in range(2, layers):
        when_inside(d, range(GROUP))
    for r, s in ((1, 1), (2, 0)):
        tok_arrived(r, s)
        share(r, s).start()
    for r in (1, 2, 3):
        arrived(1, z, at(r))
    for i in range(GROUP):
        each_way(1, z, i, start)

    @pl.when(jnp.logical_not(inside))
    def _():
        for d in range(1, layers):
            for r in range(GROUP):
                afar(d, r)

    def take(d, r):
        for layer, there in ((z - d, z - d >= 0), (z + d, z + d < layers)):
            @pl.when(there)
            def _():
                arrived(1, layer, r)
                each_way(1, layer, r, start)

    wide_n = COLS
    across = width // wide_n
    turn = jnp.where(inside, GROUP - 1, GROUP - 2)

    def first(i, carry):
        r = i // across
        b = at(r)

        @pl.when(i == turn * across)
        def _():
            for s in (0, 1):
                tok_arrived(3, s)
                share(3, s).start()

        @pl.when(i % across == 0)
        def _():
            theirs = pl.ds(pl.multiple_of(b * rows + (1 - core) * half, half), half)
            piece = tok.at[theirs, :]
            remote(piece, piece, mate_send, mate_recv.at[r], mate).wait_recv()

        m = pl.ds(pl.multiple_of(b * rows, rows), rows)
        at_n = pl.multiple_of((i % across) * wide_n, wide_n)
        pre = jnp.dot(tok[m, :], upb[:, pl.ds(at_n, wide_n)], preferred_element_type=jnp.float32)
        pre = pre * up_scale[:, pl.ds(pl.multiple_of(q * width + at_n, wide_n), wide_n)]
        hid[m, pl.ds(at_n, wide_n)] = jnp.square(jnp.maximum(pre, 0.0)).astype(hid.dtype)
        return carry

    small[1].wait()
    small[2].wait()
    lax.fori_loop(0, GROUP * across, first, 0)

    @pl.when(inside)
    def _():
        for r in range(GROUP):
            take(1, r)

    upper, lower = pl.ds(0, half), pl.ds(half, half)
    hops = ((3, upper, 2, 1), (3, lower, 2, 2), (1, upper, 0, 1), (2, lower, 1, 2),
            (1, lower, 0, 1), (2, upper, 1, 2))

    def red(u, k):
        of, part_rows, into, to = hops[k]
        return remote(
            summed.at[u, at(of), :, part_rows, :], peers.at[u, into, :, part_rows, :],
            red_send, red_recv.at[u, min(k, 2)], chip(z, at(to)),
        )

    relays = ((0, 2, upper, 5), (1, 1, lower, 4))

    def relay(u):
        for k, of, part_rows, then in relays:
            red(u, k).wait_recv()
            total = summed[u, at(of), :, part_rows, :].astype(jnp.float32)
            total = total + peers[u, 2, :, part_rows, :].astype(jnp.float32)
            summed[u, at(of), :, part_rows, :] = total.astype(summed.dtype)
            red(u, then).start()

    def unit_of(t):
        s, h = t // per_layer, t % per_layer
        layer = jnp.where(
            2 * z < layers,
            jnp.where(s <= z, z - s, s),
            jnp.where(s <= layers - 1 - z, z + s, layers - 1 - s),
        )
        unit = layer * per_layer + h
        return s, h, layer, unit, unit // (units // CORES), unit % (units // CORES)

    def part(u, b):
        return remote(
            stage.at[u, b], partner.at[u, b], part_send, part_recv.at[u, b], mate
        )

    thin = COLS // 2

    def second(t, carry):
        s, h, layer, unit, owner, u = unit_of(t)

        @pl.when(s > jnp.where(inside, 1, 0))
        def _():
            for k in range(per_unit):
                take(s, h * per_unit + k)

        cols = pl.ds(pl.multiple_of(h * COLS, COLS), COLS)
        scale = pl.ds(pl.multiple_of(unit * COLS, COLS), COLS)

        def product(b):
            m = pl.ds(pl.multiple_of(b * rows, rows), rows)
            value = jnp.dot(hid[m, :], downb[layer, :, cols], preferred_element_type=jnp.float32)
            return value * down_scale[:, scale]

        @pl.when(owner != core)
        def _():
            def away(i, c):
                b = at(GROUP - 1 - i)
                value = product(b).astype(stage.dtype)
                for e in range(2):
                    stage[u, b, e] = value[:, e * thin:(e + 1) * thin]
                part(u, b).start()
                return c

            lax.fori_loop(0, GROUP, away, 0)

        @pl.when(owner == core)
        def _():
            def mine(i, c):
                own[at(GROUP - 1 - i)] = product(at(GROUP - 1 - i))
                return c

            lax.fori_loop(0, GROUP, mine, 0)
            for r in (3, 2, 1, 0):
                b = at(r)
                part(u, b).wait_recv()
                for e in range(2):
                    total = own[b, :, e * thin:(e + 1) * thin]
                    total = total + partner[u, b, e].astype(jnp.float32)
                    summed[u, b, e] = total.astype(summed.dtype)
                for k in {3: (0, 1), 1: (2,), 2: (3,), 0: ()}[r]:
                    red(u, k).start()

        before = unit_of(jnp.maximum(t - 1, 0))

        @pl.when(jnp.logical_and(t > 0, before[4] == core))
        def _():
            relay(before[5])

        return carry

    tail = units - per_layer
    lax.fori_loop(0, tail, second, 0)
    before = unit_of(tail - 1)
    mine_end = unit_of(tail)[4] == core

    @pl.when(jnp.logical_and(before[4] == core, jnp.logical_not(mine_end)))
    def _():
        relay(before[5])

    def end_part(u, e, r):
        return remote(
            stage.at[u, at(r), e], partner.at[u, at(r), e],
            part_send, part_recv.at[u, 2 * e + (0 if r == 3 else 1)], mate,
        )

    def end_rows(k, i):
        base = hops[k][1].start
        return pl.ds(base, half) if i is None else pl.ds(base + i * sub, sub)

    def end_red(u, e, k, i=None):
        of, _, into, to = hops[k]
        come = 2 * k + i if k < 2 else 4
        return remote(
            summed.at[u, at(of), e, end_rows(k, i), :], peers.at[u, into, e, end_rows(k, i), :],
            red_send, end_red_recv.at[u % per_layer, e, come], chip(z, at(to)),
        )

    def end_relay(u, e):
        for i in range(2):
            for k, of, _, then in relays:
                end_red(u, e, k, i).wait_recv()
                total = summed[u, at(of), e, end_rows(k, i), :].astype(jnp.float32)
                total = total + peers[u, 2, e, end_rows(k, i), :].astype(jnp.float32)
                summed[u, at(of), e, end_rows(k, i), :] = total.astype(summed.dtype)
                end_red(u, e, then, i).start()

    def ending(v, carry):
        e = v % 2
        s, h, layer, unit, owner, u = unit_of(tail + v // 2)

        @pl.when(s > jnp.where(inside, 1, 0))
        def _():
            take(s, h * per_unit + e)

        cols = pl.ds(pl.multiple_of(h * COLS + e * thin, thin), thin)
        scale = pl.ds(pl.multiple_of(unit * COLS + e * thin, thin), thin)

        def product(r, into):
            for i in range(CORES):
                m = pl.ds(pl.multiple_of(at(r) * rows + i * half, half), half)
                value = jnp.dot(
                    hid[m, :], downb[layer, :, cols], preferred_element_type=jnp.float32
                )
                value = value * down_scale[:, scale]
                into[pl.ds(i * half, half), :] = value.astype(into.dtype)

        @pl.when(jnp.logical_not(mine_end))
        def _():
            for r in (3, 1, 2, 0):
                product(r, stage.at[u, at(r), e])
                end_part(u, e, r).start()

        @pl.when(mine_end)
        def _():
            def compute(r):
                product(r, own.at[r, :, pl.ds(0, thin)])

            def gather(r):
                if r == 3:
                    end_part(u, e, r).wait_recv()
                elif r == 1:
                    rest = partner.at[u, pl.ds(0, GROUP - 1), e]
                    remote(rest, rest, part_send, part_recv.at[u, 2 * e + 1], mate).wait_recv()
                total = own[r, :, :thin] + partner[u, at(r), e].astype(jnp.float32)
                summed[u, at(r), e] = total.astype(summed.dtype)
                if r == 3:
                    for i in range(2):
                        for k in range(2):
                            end_red(u, e, k, i).start()
                elif r:
                    end_red(u, e, r + 1).start()

            compute(3)
            gather(3)

            @pl.when(jnp.logical_and(v == 0, before[4] == core))
            def _():
                relay(before[5])

            @pl.when(v > 0)
            def _():
                end_relay(unit_of(tail + (v - 1) // 2)[5], (v - 1) % 2)

            compute(1)
            compute(2)
            gather(1)
            compute(0)
            gather(2)
            gather(0)

        return carry

    lax.fori_loop(0, 2 * per_layer, ending, 0)

    @pl.when(mine_end)
    def _():
        end_relay(unit_of(units - 1)[5], 1)

    def last(t, carry):
        owner, u = unit_of(t)[4:]

        @pl.when(owner == core)
        def _():
            arrive = peers.at[u, pl.ds(0, 2)]
            remote(arrive, arrive, red_send, red_recv.at[u, 2], mate).wait_recv()
            for e in range(2):
                total = summed[u, q, e].astype(jnp.float32)
                for side in range(2):
                    total = total + peers[u, side, e].astype(jnp.float32)
                at_e = pl.ds(pl.multiple_of(u * COLS + e * thin, thin), thin)
                out[:, at_e] = total.astype(out.dtype)

        return carry

    lax.fori_loop(0, tail, last, 0)

    def finish(v, carry):
        e = v % 2
        u = unit_of(tail + v // 2)[5]
        arrive = peers.at[u, pl.ds(0, 2), e]
        remote(arrive, arrive, red_send, end_red_recv.at[u % per_layer, e, 4], mate).wait_recv()
        total = summed[u, q, e].astype(jnp.float32)
        for side in range(2):
            total = total + peers[u, side, e].astype(jnp.float32)
        at_e = pl.ds(pl.multiple_of(u * COLS + e * thin, thin), thin)
        out[:, at_e] = total.astype(out.dtype)
        return carry

    def wait_sent(piece, send):
        remote(piece, piece, send, piece_recv.at[0, 0], mate).wait_send()

    def drain_early():
        for kind in (0, 1):
            wait_sent(upb.at[pl.ds(0, (GROUP - 1) * depth), :], level_send.at[kind])
        wait_sent(tok.at[pl.ds(0, 6 * sub), :], tok_send)
        wait_sent(tok.at[pl.ds(0, 2 * GROUP * sub), :], mate_send)
        for at_z in range(layers):
            @pl.when(z == at_z)
            def _():
                for way, reach in ((1, at_z + 1), (0, layers - at_z)):
                    if (way and at_z < layers - 1) or (not way and at_z > 0):
                        pieces = upb.at[pl.ds(0, reach * GROUP * depth), :]
                        wait_sent(pieces, piece_send.at[0, way])
                        wait_sent(downb.at[pl.ds(0, reach)], piece_send.at[1, way])

    drain_early()
    wait_sent(stage, part_send)

    @pl.when(mine_end)
    def _():
        lax.fori_loop(0, 2 * per_layer, finish, 0)

    wait_sent(peers, red_send)


def grouped(layers, tokens, norm_gain, up_weight, up_scale, down_weight, down_scale):
    rows, model = tokens.shape
    depth = up_weight.shape[0]
    if 2 * depth != COLS:
        return gathered(
            tokens, norm_gain, up_weight, up_scale, down_weight, down_scale
        )
    width = up_weight.shape[1] // GROUP
    share = model // COLS // CORES
    n = layers * GROUP
    dma = pltpu.SemaphoreType.DMA
    vmem = pl.BlockSpec(memory_space=pltpu.VMEM)
    hbm = pl.BlockSpec(memory_space=pltpu.HBM)
    ff = up_weight.shape[1]
    return pl.pallas_call(
        functools.partial(layer_kernel, layers, rows),
        out_shape=pltpu.VMEM((rows, model // CORES), jnp.bfloat16),
        in_specs=[hbm] * 6,
        out_specs=vmem,
        scratch_shapes=[
            pltpu.VMEM((1, model), jnp.float32),
            pltpu.VMEM((1, ff), jnp.float32),
            pltpu.VMEM((1, model), jnp.float32),
            pltpu.VMEM((GROUP * rows, model), jnp.bfloat16),
            pltpu.VMEM((model, width), jnp.bfloat16),
            pltpu.VMEM((layers, width, GROUP * depth), jnp.bfloat16),
            pltpu.VMEM((GROUP * rows, width), jnp.bfloat16),
            pltpu.VMEM((share, GROUP, 2, rows, COLS // 2), jnp.bfloat16),
            pltpu.VMEM((share, GROUP, 2, rows, COLS // 2), jnp.bfloat16),
            pltpu.VMEM((share, GROUP, 2, rows, COLS // 2), jnp.bfloat16),
            pltpu.VMEM((share, GROUP - 1, 2, rows, COLS // 2), jnp.bfloat16),
            pltpu.VMEM((GROUP, rows, COLS), jnp.float32),
            pltpu.VMEM((depth, GROUP * width), jnp.float32),
            pltpu.VMEM((GROUP * width, depth), jnp.float32),
            pltpu.VMEM((GROUP, depth, width), jnp.bfloat16),
            pltpu.VMEM((GROUP, width, depth), jnp.bfloat16),
            dma((7,)),
            dma((2, n)),
            dma((2, 2)),
            dma((2,)),
            dma((GROUP - 1, 2)),
            dma((GROUP - 1, 2)),
            dma((GROUP,)),
            dma((share, GROUP)),
            dma((share, 3)),
            dma((2, 2, 5)),
            dma((4,)),
        ],
        compiler_params=pltpu.CompilerParams(
            collective_id=0, has_side_effects=True, vmem_limit_bytes=60 * 2**20
        ),
    )(
        tokens, norm_gain.reshape(1, -1), up_weight, down_weight, up_scale.reshape(1, -1), down_scale
    )


def solution(mesh):
    fs, tp = mesh.shape["fs"], mesh.shape["tp"]
    if tp == CORES and fs % (2 * GROUP) == 0 and fs <= 4 * GROUP:
        body = functools.partial(grouped, fs // GROUP)
    else:
        body = gathered
    in_specs = (P("fs", None), P(), P("fs", "tp"), P("tp"), P("tp", "fs"), P())
    out_specs = P("fs", "tp")
    return jax.shard_map(
        body, mesh=mesh, in_specs=in_specs, out_specs=out_specs, check_vma=False
    )
```

time: 159 us -> 150 us (0.943)
  Pallas kernels: 157 us -> 149 us
    pallas_call x1, Pallas kernels: 157 us -> 149 us  [grouped(): pl.pallas_call(functools.partial(layer_kernel, layers, rows), out_shape=p...]
where the time goes in v2:
time: 150 us
  Pallas kernels  149 us (99%)
    pallas_call x1, Pallas kernels, grouped(): pl.pallas_call(functools.partial(layer_kernel, layers, rows), out_shape=p...  149 us

profile of v2, /device:TPU:1, one launch (start us, length us, event | category | flops | bytes accessed | tf_op | source)
XLA Modules:
  0.0 150.3 jit_solution(2358930121383348022)
XLA Ops:
  0.0 149.2 %shard_map.64 = bf16[768,1024]{1,0:T(8,128)(2,1)S(1)} custom-call(bf16[768,2048]{1,0:T(8,128)(2,1)} %tokens.1, f32[1,2048]{1,0:T(1,128)} %bitcast.3, f32[128,4096]{1,0:T(8,128)} %up_in.1, f32[4096,128]{1,0:T(8,128)} %down_in.1, f32[1,4096]{1,0:T(1,128)} %bitcast.2, f32[1,2048]{1,0:T(1,128)} %down_scale_in.1), custom_call_target="tpu_custom_call" | custom-call | tf_op jit(solution)/shard_map/pallas_call | solution.py:601
  149.2 1.1 copy.8

commit v3 on v2

--- a/solution.py
+++ b/solution.py
@@ -61,7 +61,7 @@
     mate = (fs, 1 - core)
 
     barrier = pltpu.get_barrier_semaphore()
-    for r in range(1, GROUP):
+    for r in (1, 2):
         pl.semaphore_signal(barrier, inc=1, device_id=chip(z, at(r)), device_id_type=MESH)
     pl.semaphore_signal(barrier, inc=1, device_id=mate, device_id_type=MESH)
 
@@ -192,7 +192,7 @@
     up_copy(0).wait()
     own_rows = pl.ds(pl.multiple_of(fs * depth, depth), depth)
     upb[own_rows, :] = up_wide[:, part_at(0)].astype(upb.dtype)
-    greeted = GROUP + jnp.where(z > 0, 1, 0) + jnp.where(z < layers - 1, 1, 0)
+    greeted = GROUP - 1 + jnp.where(z > 0, 1, 0) + jnp.where(z < layers - 1, 1, 0)
     pl.semaphore_wait(barrier, greeted)
     each_way(0, z, q, start)
     others = up_wide.at[:, pl.ds(0, (GROUP - 1) * width)]
@@ -200,7 +200,7 @@
     for r in range(1, GROUP):
         up_cast[at(r)] = up_wide[:, part_at(r)].astype(up_cast.dtype)
 
-    for r in (1, 2, 3):
+    for r in (1, 2):
         for h in (0, 1):
             near_half(r, h).start()
 
@@ -214,20 +214,11 @@
     token_copy.wait()
     small[0].wait()
     lax.fori_loop(0, half // STRIP, normalize, 0)
-
-    hand(1, 0).start()
-    hand(2, 1).start()
-    hand(1, 1).start()
-    hand(2, 0).start()
     down_copy.wait()
     own_cols = pl.ds(pl.multiple_of(q * depth, depth), depth)
     downb[z, :, own_cols] = down_wide[part_at(0), :].astype(downb.dtype)
     for r in range(1, GROUP):
         down_cast[at(r)] = down_wide[part_at(r), :].astype(down_cast.dtype)
-    for r in (1, 2, 3):
-        level(r).start()
-    for s in (0, 1):
-        share(0, s).start()
 
     inside = jnp.logical_and(z > 0, z < layers - 1)
 
@@ -256,9 +247,20 @@
             for r in rs:
                 afar(d, r)
 
+    near(1, 0)
     for h in (0, 1):
-        for r in (1, 2):
-            near(r, h)
+        near_half(3, h).start()
+    hand(1, 0).start()
+    hand(2, 1).start()
+    hand(1, 1).start()
+    hand(2, 0).start()
+    for r in (1, 2, 3):
+        level(r).start()
+    for s in (0, 1):
+        share(0, s).start()
+    near(2, 0)
+    near(1, 1)
+    near(2, 1)
     when_inside(1, (0,))
     for h in (0, 1):
         near(3, h)
@@ -290,8 +292,14 @@
             @pl.when(there)
             def _():
                 arrived(1, layer, r)
-                each_way(1, layer, r, start)
-
+
+                @pl.when(jnp.logical_not(jnp.logical_and(
+                    holds, jnp.logical_and(layer == layers - 1, r == GROUP - 1)
+                )))
+                def _():
+                    each_way(1, layer, r, start)
+
+    holds = jnp.logical_and(core == 1, jnp.logical_and(inside, z == 1))
     wide_n = COLS
     across = width // wide_n
     turn = jnp.where(inside, GROUP - 1, GROUP - 2)
@@ -457,6 +465,11 @@
 
     def ending(v, carry):
         e = v % 2
+
+        @pl.when(jnp.logical_and(holds, v == 2 * per_layer - 1))
+        def _():
+            each_way(1, layers - 1, GROUP - 1, start)
+
         s, h, layer, unit, owner, u = unit_of(tail + v // 2)
 
         @pl.when(s > jnp.where(inside, 1, 0))

time: 150 us -> 149 us (level)
    pallas_call x1, Pallas kernels: 149 us -> 148 us  [grouped(): pl.pallas_call(functools.partial(layer_kernel, layers, rows), out_shape=p...]
where the time goes in v3:
time: 149 us
  Pallas kernels  148 us (99%)
    pallas_call x1, Pallas kernels, grouped(): pl.pallas_call(functools.partial(layer_kernel, layers, rows), out_shape=p...  148 us

profile of v3, /device:TPU:1, one launch (start us, length us, event | category | flops | bytes accessed | tf_op | source)
XLA Modules:
  0.0 148.8 jit_solution(10529620241748766010)
XLA Ops:
  0.0 147.6 %shard_map.64 = bf16[768,1024]{1,0:T(8,128)(2,1)S(1)} custom-call(bf16[768,2048]{1,0:T(8,128)(2,1)} %tokens.1, f32[1,2048]{1,0:T(1,128)} %bitcast.3, f32[128,4096]{1,0:T(8,128)} %up_in.1, f32[4096,128]{1,0:T(8,128)} %down_in.1, f32[1,4096]{1,0:T(1,128)} %bitcast.2, f32[1,2048]{1,0:T(1,128)} %down_scale_in.1), custom_call_target="tpu_custom_call" | custom-call | tf_op jit(solution)/shard_map/pallas_call | solution.py:614
  147.6 1.1 copy.8

commit v4 on v3

--- a/solution.py
+++ b/solution.py
@@ -287,6 +287,19 @@
             for r in range(GROUP):
                 afar(d, r)
 
+    def unit_of(t):
+        s, h = t // per_layer, t % per_layer
+        layer = jnp.where(
+            2 * z < layers,
+            jnp.where(s <= z, z - s, s),
+            jnp.where(s <= layers - 1 - z, z + s, layers - 1 - s),
+        )
+        unit = layer * per_layer + h
+        return s, h, layer, unit, unit // (units // CORES), unit % (units // CORES)
+
+    mine_end = unit_of(units - per_layer)[4] == core
+    holds = jnp.logical_and(mine_end, jnp.logical_and(inside, z == 1))
+
     def take(d, r):
         for layer, there in ((z - d, z - d >= 0), (z + d, z + d < layers)):
             @pl.when(there)
@@ -299,7 +312,6 @@
                 def _():
                     each_way(1, layer, r, start)
 
-    holds = jnp.logical_and(core == 1, jnp.logical_and(inside, z == 1))
     wide_n = COLS
     across = width // wide_n
     turn = jnp.where(inside, GROUP - 1, GROUP - 2)
@@ -356,16 +368,6 @@
             total = total + peers[u, 2, :, part_rows, :].astype(jnp.float32)
             summed[u, at(of), :, part_rows, :] = total.astype(summed.dtype)
             red(u, then).start()
-
-    def unit_of(t):
-        s, h = t // per_layer, t % per_layer
-        layer = jnp.where(
-            2 * z < layers,
-            jnp.where(s <= z, z - s, s),
-            jnp.where(s <= layers - 1 - z, z + s, layers - 1 - s),
-        )
-        unit = layer * per_layer + h
-        return s, h, layer, unit, unit // (units // CORES), unit % (units // CORES)
 
     def part(u, b):
         return remote(
@@ -430,7 +432,6 @@
     tail = units - per_layer
     lax.fori_loop(0, tail, second, 0)
     before = unit_of(tail - 1)
-    mine_end = unit_of(tail)[4] == core
 
     @pl.when(jnp.logical_and(before[4] == core, jnp.logical_not(mine_end)))
     def _():
@@ -466,9 +467,13 @@
     def ending(v, carry):
         e = v % 2
 
-        @pl.when(jnp.logical_and(holds, v == 2 * per_layer - 1))
-        def _():
-            each_way(1, layers - 1, GROUP - 1, start)
+        def release(when):
+            @pl.when(jnp.logical_and(when, jnp.logical_and(holds, v == 2 * per_layer - 1)))
+            def _():
+                each_way(1, layers - 1, GROUP - 1, start)
+
+        corner = q == GROUP - 1
+        release(jnp.logical_not(corner))
 
         s, h, layer, unit, owner, u = unit_of(tail + v // 2)
 
@@ -516,6 +521,7 @@
 
             compute(3)
             gather(3)
+            release(corner)
 
             @pl.when(jnp.logical_and(v == 0, before[4] == core))
             def _():

time: 149 us -> 149 us (level)
  no operation moved by 1% of the time
where the time goes in v4:
time: 149 us
  Pallas kernels  147 us (99%)
    pallas_call x1, Pallas kernels, grouped(): pl.pallas_call(functools.partial(layer_kernel, layers, rows), out_shape=p...  147 us

profile of v4, /device:TPU:1, one launch (start us, length us, event | category | flops | bytes accessed | tf_op | source)
XLA Modules:
  0.0 148.5 jit_solution(3156675390146222431)
XLA Ops:
  0.0 147.3 %shard_map.64 = bf16[768,1024]{1,0:T(8,128)(2,1)S(1)} custom-call(bf16[768,2048]{1,0:T(8,128)(2,1)} %tokens.1, f32[1,2048]{1,0:T(1,128)} %bitcast.3, f32[128,4096]{1,0:T(8,128)} %up_in.1, f32[4096,128]{1,0:T(8,128)} %down_in.1, f32[1,4096]{1,0:T(1,128)} %bitcast.2, f32[1,2048]{1,0:T(1,128)} %down_scale_in.1), custom_call_target="tpu_custom_call" | custom-call | tf_op jit(solution)/shard_map/pallas_call | solution.py:620
  147.4 1.1 copy.8

commit v5 on v4

--- a/solution.py
+++ b/solution.py
@@ -519,18 +519,17 @@
                 elif r:
                     end_red(u, e, r + 1).start()
 
+            @pl.when(jnp.logical_and(v == 0, before[4] == core))
+            def _():
+                relay(before[5])
+
+            @pl.when(v > 0)
+            def _():
+                end_relay(unit_of(tail + (v - 1) // 2)[5], (v - 1) % 2)
+
             compute(3)
             gather(3)
             release(corner)
-
-            @pl.when(jnp.logical_and(v == 0, before[4] == core))
-            def _():
-                relay(before[5])
-
-            @pl.when(v > 0)
-            def _():
-                end_relay(unit_of(tail + (v - 1) // 2)[5], (v - 1) % 2)
-
             compute(1)
             compute(2)
             gather(1)

time: 149 us -> 151 us (1.013)
  Pallas kernels: 147 us -> 150 us
    pallas_call x1, Pallas kernels: 147 us -> 150 us  [grouped(): pl.pallas_call(functools.partial(layer_kernel, layers, rows), out_shape=p...]
where the time goes in v5:
time: 151 us
  Pallas kernels  150 us (99%)
    pallas_call x1, Pallas kernels, grouped(): pl.pallas_call(functools.partial(layer_kernel, layers, rows), out_shape=p...  150 us

profile of v5, /device:TPU:1, one launch (start us, length us, event | category | flops | bytes accessed | tf_op | source)
XLA Modules:
  0.0 150.9 jit_solution(12743171439862468425)
XLA Ops:
  0.0 149.7 %shard_map.64 = bf16[768,1024]{1,0:T(8,128)(2,1)S(1)} custom-call(bf16[768,2048]{1,0:T(8,128)(2,1)} %tokens.1, f32[1,2048]{1,0:T(1,128)} %bitcast.3, f32[128,4096]{1,0:T(8,128)} %up_in.1, f32[4096,128]{1,0:T(8,128)} %down_in.1, f32[1,4096]{1,0:T(1,128)} %bitcast.2, f32[1,2048]{1,0:T(1,128)} %down_scale_in.1), custom_call_target="tpu_custom_call" | custom-call | tf_op jit(solution)/shard_map/pallas_call | solution.py:619
  149.7 1.1 copy.8
